TPU v7x, 32 devices: a whole 2x2x4 slice. The times are simulated.
32 devices in a mesh: ep: 8 (over z, core), tp: 4 (over y, x).
Axes of the slice: x: 2, y: 2, z: 4, core: 2. Of those that a mesh axis runs over, the one named last changes fastest.
Arguments:
- tokens: bfloat16 [512, 2048], P('ep'), may hold values from -6 to 6
- mix_gain: float32 [2048], replicated, may hold values from 0.1 to 1.9
- w_in: bfloat16 [2048, 1024], P(None, 'tp'), may hold values from -0.125 to 0.125
- decay_re: float32 [64, 64], P('tp'), may hold values from -1 to -0.1
- freq: float32 [64, 64], P('tp'), may hold values from 0 to 100
- log_step: float32 [64], P('tp'), may hold values from -3.9 to 0
- in_re: bfloat16 [64, 16, 64], P('tp'), may hold values from -1 to 1
- in_im: bfloat16 [64, 16, 64], P('tp'), may hold values from -1 to 1
- out_re: bfloat16 [64, 16, 64], P('tp'), may hold values from -0.75 to 0.75
- out_im: bfloat16 [64, 16, 64], P('tp'), may hold values from -0.75 to 0.75
- skip: float32 [64, 16], P('tp'), may hold values from -4 to 4
- state_re: float32 [512, 64, 64], P('ep', 'tp'), may hold values from -6 to 6
- state_im: float32 [512, 64, 64], P('ep', 'tp'), may hold values from -6 to 6
- glu_weight: bfloat16 [1024, 1024], P(None, 'tp'), may hold values from -0.1875 to 0.1875
- glu_bias: float32 [1024], P('tp'), may hold values from -4 to 4
- out_weight: bfloat16 [1024, 2048], P('tp'), may hold values from -0.1875 to 0.1875
- ffn_gain: float32 [2048], replicated, may hold values from 0.1 to 1.9
- route: int32 [512, 2], P('ep'), may hold values from 0 to 7, all different within a row; in each aligned block of 64 rows (0 to 63, 64 to 127, ...) at most 24 rows name the same one
- route_weight: float32 [512, 2], P('ep'), may hold values from 0.2 to 1
- expert_gate: bfloat16 [8, 2048, 3584], P('ep', None, 'tp'), may hold values from -0.125 to 0.125
- expert_up: bfloat16 [8, 2048, 3584], P('ep', None, 'tp'), may hold values from -0.125 to 0.125
- expert_down: bfloat16 [8, 3584, 2048], P('ep', 'tp'), may hold values from -0.09375 to 0.09375
Outputs:
- mixed: bfloat16 [512, 2048], P('ep', 'tp')
- new_re: float32 [512, 64, 64], P('ep', 'tp')
- new_im: float32 [512, 64, 64], P('ep', 'tp')
Inputs may be any that keep to these rules, and one draw needn't show every extreme that they name: `route`: each row names 2 different experts. Within the 64 rows of one index of ep no expert is named more than 24 times, and in every draw some expert is named exactly 24 times by the rows of some index of ep.
All inputs are finite; a program needn't handle non-finite values.
Results may differ from a plain program's by a relative error of at most 0.015.
Values may be sent and summed in bfloat16 or wider, within the bound.
A program may use at most 64 MiB of HBM per device.

v0:
```python
import jax
import jax.numpy as jnp
from jax import lax
from jax.sharding import PartitionSpec as P

norm_eps = 1e-06


def rms_scale(rows, gain):
    values = rows.astype(jnp.float32)
    scaled = values * lax.rsqrt(jnp.mean(values * values, axis=-1, keepdims=True) + norm_eps)
    return (scaled * gain).astype(jnp.bfloat16)


def state_step(
    inputs, state_re, state_im, decay_re, freq, log_step, in_re, in_im, out_re, out_im, skip
):
    highest = lax.Precision.HIGHEST
    step = jnp.exp(log_step)[:, None]
    magnitude = jnp.exp(decay_re * step)
    turn_re = magnitude * jnp.cos(freq * step)
    turn_im = magnitude * jnp.sin(freq * step)
    denom = decay_re * decay_re + freq * freq
    coef_re = ((turn_re - 1.0) * decay_re + turn_im * freq) / denom
    coef_im = (turn_im * decay_re - (turn_re - 1.0) * freq) / denom
    drive_re = jnp.einsum("sgh,ghp->sgp", inputs, in_re, preferred_element_type=jnp.float32)
    drive_im = jnp.einsum("sgh,ghp->sgp", inputs, in_im, preferred_element_type=jnp.float32)
    push_re = coef_re * drive_re - coef_im * drive_im
    push_im = coef_re * drive_im + coef_im * drive_re
    new_re = turn_re * state_re - turn_im * state_im + push_re
    new_im = turn_re * state_im + turn_im * state_re + push_im
    read = jnp.einsum("ghp,sgp->sgh", out_re.astype(jnp.float32), new_re, precision=highest)
    read = read - jnp.einsum("ghp,sgp->sgh", out_im.astype(jnp.float32), new_im, precision=highest)
    read = read + skip * inputs.astype(jnp.float32)
    return (read, new_re, new_im)


def local(
    tokens,
    mix_gain,
    w_in,
    decay_re,
    freq,
    log_step,
    in_re,
    in_im,
    out_re,
    out_im,
    skip,
    state_re,
    state_im,
    glu_weight,
    glu_bias,
    out_weight,
    ffn_gain,
    route,
    route_weight,
    expert_gate,
    expert_up,
    expert_down,
):
    seq_count = tokens.shape[0]
    groups_local = decay_re.shape[0]
    model_width = tokens.shape[1]
    local_width = model_width // lax.axis_size("tp")
    experts = lax.axis_size("ep")
    top_count = route.shape[1]
    slot_cap = (3 * seq_count * top_count + 2 * experts - 1) // (2 * experts)
    col_start = lax.axis_index("tp") * local_width
    normed = rms_scale(tokens, mix_gain)
    drive = jnp.dot(normed, w_in, preferred_element_type=jnp.float32).astype(jnp.bfloat16)
    inputs = drive.reshape(seq_count, groups_local, -1)
    read, new_re, new_im = state_step(
        inputs, state_re, state_im, decay_re, freq, log_step, in_re, in_im, out_re, out_im, skip
    )
    mixed_in = jax.nn.gelu(read).reshape(seq_count, -1).astype(jnp.bfloat16)
    gate = jnp.dot(
        lax.all_gather(mixed_in, "tp", axis=1, tiled=True),
        glu_weight,
        preferred_element_type=jnp.float32,
    )
    gated = (mixed_in.astype(jnp.float32) * jax.nn.sigmoid(gate + glu_bias)).astype(jnp.bfloat16)
    partial_value = jnp.dot(gated, out_weight, preferred_element_type=jnp.float32)
    mix_part = lax.psum_scatter(
        partial_value.astype(jnp.bfloat16), "tp", scatter_dimension=1, tiled=True
    ).astype(jnp.float32)
    token_part = lax.dynamic_slice_in_dim(tokens, col_start, local_width, 1)
    resid_part = (token_part.astype(jnp.float32) + mix_part).astype(jnp.bfloat16)
    part_values = resid_part.astype(jnp.float32)
    squares = lax.psum(jnp.sum(part_values * part_values, axis=1), "tp")
    row_scale = lax.rsqrt(squares / model_width + norm_eps)
    gain_part = lax.dynamic_slice_in_dim(ffn_gain, col_start, local_width, 0)
    own_cols = (part_values * row_scale[:, None] * gain_part).astype(jnp.bfloat16)
    flat_route = route.reshape(-1)
    hits = (flat_route[:, None] == jnp.arange(experts)[None, :]).astype(jnp.int32)
    rank = jnp.sum((jnp.cumsum(hits, axis=0) - hits) * hits, axis=1)
    slot = flat_route * slot_cap + rank
    slot_ids = jnp.arange(experts * slot_cap)
    picks = (slot[None, :] == slot_ids[:, None]).reshape(experts * slot_cap, seq_count, top_count)
    select = jnp.any(picks, axis=2).astype(jnp.bfloat16)
    combine = jnp.einsum("ask,sk->sa", picks.astype(jnp.float32), route_weight)
    gate_local = expert_gate[0]
    up_local = expert_up[0]
    down_local = expert_down[0]
    normed2 = lax.all_gather(own_cols, "tp", axis=1, tiled=True)
    outbound = jnp.dot(select, normed2, preferred_element_type=jnp.float32).astype(jnp.bfloat16)
    arrived = lax.all_to_all(
        outbound.reshape(experts, slot_cap, model_width),
        "ep",
        split_axis=0,
        concat_axis=0,
        tiled=True,
    )
    arrived = arrived.reshape(experts * slot_cap, model_width)
    gate_rows = jnp.dot(arrived, gate_local, preferred_element_type=jnp.float32)
    up_rows = jnp.dot(arrived, up_local, preferred_element_type=jnp.float32)
    hidden = (jax.nn.silu(gate_rows) * up_rows).astype(jnp.bfloat16)
    back_rows = lax.psum_scatter(
        lax.dot_general(
            down_local, hidden, (((0,), (1,)), ((), ())), preferred_element_type=jnp.float32
        ).astype(jnp.bfloat16),
        "tp",
        scatter_dimension=0,
        tiled=True,
    ).astype(jnp.float32)
    back_rows = back_rows.astype(jnp.bfloat16).reshape(local_width, experts, slot_cap)
    returned = lax.all_to_all(back_rows, "ep", split_axis=1, concat_axis=1, tiled=True)
    returned = returned.reshape(local_width, experts * slot_cap).astype(jnp.float32)
    expert_total = lax.dot_general(
        combine, returned, (((1,), (1,)), ((), ())), precision=lax.Precision.HIGHEST
    )
    mixed = (resid_part.astype(jnp.float32) + expert_total).astype(jnp.bfloat16)
    return (mixed, new_re, new_im)


def solution(mesh):
    in_specs = (
        P("ep", None),
        P(),
        P(None, "tp"),
        P("tp", None),
        P("tp", None),
        P("tp"),
        P("tp", None, None),
        P("tp", None, None),
        P("tp", None, None),
        P("tp", None, None),
        P("tp", None),
        P("ep", "tp", None),
        P("ep", "tp", None),
        P(None, "tp"),
        P("tp"),
        P("tp", None),
        P(),
        P("ep", None),
        P("ep", None),
        P("ep", None, "tp"),
        P("ep", None, "tp"),
        P("ep", "tp", None),
    )
    out_specs = (P("ep", "tp"), P("ep", "tp", None), P("ep", "tp", None))
    return jax.shard_map(local, mesh=mesh, in_specs=in_specs, out_specs=out_specs, check_vma=False)
```

profile of v0, /device:TPU:0, one launch (start us, length us, event | category | flops | bytes accessed | tf_op | source)
XLA Modules:
  0.0 152.2 jit_solution(17979574548107421040)
XLA Ops:
  7.2 0.0 copy-start
  7.2 0.0 copy-start.2
  7.2 0.0 copy-start.3
  7.2 0.0 copy-start.4
  7.2 0.0 copy-start.1
  7.2 0.0 copy-start.6
  7.2 0.0 reduce-scatter.3.cloned.1.call-start
  7.3 0.8 exp.13
  8.0 1.1 fusion.34
  9.2 1.7 %convolution_convert_fusion.2 = bf16[64,256]{1,0:T(8,128)(2,1)S(1)} fusion(bf16[2048,256]{1,0:T(8,128)(2,1)} %param.24, bf16[64,2048]{1,0:T(8,128)(2,1)} %param.22, f32[2048]{0:T(1024)} %param.23, f32[64]{0:T(128)S(1)} %add_rsqrt_fusion.1), kind=kOutput, calls=%fused_computation.24 | convolution fusion | flops 67649536 | bytes 1351936 | tf_op jit(solution)/shard_map/dot_general | solution.py:71
  10.8 0.1 copy.61
  11.0 1.1 fusion.64
  12.1 0.0 copy-start.5
  12.1 0.8 cosine_multiply_fusion
  12.9 1.8 %bitcast_add_fusion = (f32[64,16,64]{2,0,1:T(8,128)S(1)}, f32[64,16,64]{2,0,1:T(8,128)S(1)}) fusion(f32[16,64,64]{2,1,0:T(8,128)S(1)} %fusion.64, f32[64,16,64]{2,1,0:T(8,128)} %param.34, f32[64,16,64]{2,1,0:T(8,128)} %param.33, f32[16,64]{1,0:T(8,128)S(1)} %get-tuple-element.21, f32[16,64]{1,0:T(8,128)S(1)} %get-tuple-element.22, ...), kind=kOutput, calls=%fused_computation.35 | convolution fusion | flops 3014656 | bytes 1392640 | tf_op jit(solution)/shard_map/sgh,ghp->sgp/dot_general | solution.py:26
  14.7 0.0 copy-done.2
  14.7 0.5 fusion.65
  15.2 0.0 copy-done.3
  15.2 0.0 copy-done.4
  15.2 0.5 fusion.50
  15.8 10.5 %all_gather.6 = bf16[64,1024]{0,1:T(8,128)(2,1)S(1)} all-gather(bf16[64,256]{0,1:T(8,128)(2,1)S(1)} %bitcast.68), channel_id=1, replica_groups=mesh['ep'=8,'tp'=4] {'tp'}, dimensions={1}, use_global_device_ids=true | all-gather | bytes 163840 | tf_op jit(solution)/shard_map/all_gather | solution.py:78
  26.3 0.1 copy.64
  26.4 0.0 copy-done
  26.4 0.0 copy-done.1
  26.4 0.0 copy-done.6
  26.4 1.3 convolution_convert_fusion.1
  27.7 0.0 reduce-scatter.3.cloned.1.call-update
  27.8 0.0 reduce-scatter.5.cloned.1.call-start
  27.8 0.0 copy-done.5
  27.8 0.1 copy.65
  27.9 0.1 eq.29
  28.1 0.1 fusion.56
  28.2 0.2 reduce_window_sum.11
  28.3 0.2 select_reduce_fusion
  28.5 0.1 reduce_sum.31
  28.6 0.1 copy.66
  28.7 0.8 dynamic_slice.7
  29.5 0.1 iota_compare_fusion
  29.6 22.9 %reduce-scatter.3.cloned.1.call-done = bf16[64,512]{1,0:T(8,128)(2,1)} async-done(((bf16[64,2048]{1,0:T(8,128)(2,1)}), bf16[64,512]{1,0:T(8,128)(2,1)}) %reduce-scatter.3.cloned.1.call-update) | async-done | bytes 65552 | tf_op jit(solution)/shard_map/reduce_scatter | solution.py:84
  52.5 1.0 fusion.51
  53.5 8.9 %psum.7 = f32[64]{0:T(128)S(1)} all-reduce(f32[64]{0:T(128)S(1)} %get-tuple-element.15), channel_id=1, replica_groups=mesh['ep'=8,'tp'=4] {'tp'}, use_global_device_ids=true, to_apply=%region_6.7 | all-reduce | flops 64 | bytes 512 | tf_op jit(solution)/shard_map/psum | solution.py:90
  62.5 0.1 fusion.53
  62.6 8.9 %all_gather.7 = bf16[64,2048]{1,0:T(8,128)(2,1)S(1)} all-gather(bf16[64,512]{1,0:T(8,128)(2,1)S(1)} %fusion.53), channel_id=1, replica_groups=mesh['ep'=8,'tp'=4] {'tp'}, dimensions={1}, use_global_device_ids=true | all-gather | bytes 327680 | tf_op jit(solution)/shard_map/all_gather | solution.py:105
  71.5 0.4 convolution_convert_fusion
  71.9 25.4 %all_to_all.10 = bf16[8,24,2048]{2,1,0:T(8,128)(2,1)S(1)} all-to-all(bf16[8,24,2048]{2,1,0:T(8,128)(2,1)S(1)} %bitcast.63), channel_id=1, replica_groups=mesh['ep'=8,'tp'=4] {'ep'}, dimensions={0} | all-to-all | bytes 1572864 | tf_op jit(solution)/shard_map/all_to_all | solution.py:107
  97.3 3.9 %fusion.4 = f32[192,896]{1,0:T(8,128)} fusion(bf16[192,2048]{1,0:T(8,128)(2,1)S(1)} %bitcast.61, bf16[1,2048,896]{2,1,0:T(8,128)(2,1)} %param.41), kind=kOutput, calls=%fused_computation.4 | convolution fusion | flops 704643072 | bytes 5144576 | tf_op jit(solution)/shard_map/dot_general | solution.py:115
  101.2 0.0 copy-start.7
  101.2 6.1 %fusion.9 = bf16[2048,192]{0,1:T(8,128)(2,1)} fusion(bf16[1,896,2048]{2,1,0:T(8,128)(2,1)} %param.43, bf16[192,2048]{1,0:T(8,128)(2,1)S(1)} %bitcast.62, bf16[1,2048,896]{2,1,0:T(8,128)(2,1)} %param.42, f32[192,896]{1,0:T(8,128)} %fusion.4), kind=kOutput, calls=%fused_computation.8 | convolution fusion | flops 1410711552 | bytes 9601024 | tf_op jit(solution)/shard_map/dot_general | solution.py:119
  107.3 0.0 reduce-scatter.5.cloned.1.call-update
  107.3 24.3 %reduce-scatter.5.cloned.1.call-done = bf16[512,192]{0,1:T(8,128)(2,1)} async-done(((bf16[2048,192]{0,1:T(8,128)(2,1)}), bf16[512,192]{0,1:T(8,128)(2,1)}) %reduce-scatter.5.cloned.1.call-update) | async-done | bytes 196624 | tf_op jit(solution)/shard_map/reduce_scatter | solution.py:118
  131.6 4.6 %all-to-all-start.1 = ((bf16[512,8,24]{0,2,1:T(8,128)(2,1)}), bf16[512,8,24]{0,2,1:T(8,128)(2,1)S(1)}, u32[]{:S(2)}, u32[]{:S(2)}) async-start(bf16[512,8,24]{0,2,1:T(8,128)(2,1)} %bitcast.70), calls=%async_computation.3 | async-start | bytes 393216 | tf_op jit(solution)/shard_map/all_to_all | solution.py:127
  136.2 1.1 copy.67
  137.3 1.1 copy.68
  138.4 0.0 copy-done.7
  138.4 0.1 copy.70
  138.5 0.2 fusion.41
  138.7 5.7 %all-to-all-done.1 = bf16[512,8,24]{0,2,1:T(8,128)(2,1)S(1)} async-done(((bf16[512,8,24]{0,2,1:T(8,128)(2,1)}), bf16[512,8,24]{0,2,1:T(8,128)(2,1)S(1)}, u32[]{:S(2)}, u32[]{:S(2)}) %all-to-all-start.1) | async-done | bytes 196640 | tf_op jit(solution)/shard_map/all_to_all | solution.py:127
  144.5 0.9 fusion.20
  (3 shorter events, 0.0 us)
Async XLA Ops:
  7.2 19.2 %copy-start = (bf16[256,2048]{1,0:T(8,128)(2,1)S(1)}, bf16[256,2048]{1,0:T(8,128)(2,1)}, u32[]{:S(2)}) copy-start(bf16[256,2048]{1,0:T(8,128)(2,1)} %param.37) | copy-start | bytes 3145732
  7.2 7.5 %copy-start.2 = (bf16[16,16,64]{2,1,0:T(8,128)(2,1)S(1)}, bf16[16,16,64]{2,1,0:T(8,128)(2,1)}, u32[]{:S(2)}) copy-start(bf16[16,16,64]{2,1,0:T(8,128)(2,1)} %param.30) | copy-start | bytes 98308
  7.2 8.0 %copy-start.3 = (bf16[16,16,64]{2,1,0:T(8,128)(2,1)S(1)}, bf16[16,16,64]{2,1,0:T(8,128)(2,1)}, u32[]{:S(2)}) copy-start(bf16[16,16,64]{2,1,0:T(8,128)(2,1)} %param.31) | copy-start | bytes 98308
  7.2 8.0 %copy-start.4 = (f32[16,16]{1,0:T(8,128)S(1)}, f32[16,16]{1,0:T(8,128)}, u32[]{:S(2)}) copy-start(f32[16,16]{1,0:T(8,128)} %param.32) | copy-start | bytes 3076
  7.2 19.2 %copy-start.1 = (bf16[1024,256]{1,0:T(8,128)(2,1)S(1)}, bf16[1024,256]{1,0:T(8,128)(2,1)}, u32[]{:S(2)}) copy-start(bf16[1024,256]{1,0:T(8,128)(2,1)} %param.35) | copy-start | bytes 1572868
  7.2 19.2 %copy-start.6 = (f32[256]{0:T(256)S(1)}, f32[256]{0:T(256)}, u32[]{:S(2)}) copy-start(f32[256]{0:T(256)} %param.36) | copy-start | bytes 3076
  7.2 45.3 %reduce-scatter.3.cloned.1.call-start = ((), (), s32[]{:S(2)}) async-start(), calls=%async_computation.4 | async-start | bytes 327680 | tf_op jit(solution)/shard_map/reduce_scatter | solution.py:84
  12.1 15.7 %copy-start.5 = (s32[64,2]{0,1:T(2,128)S(1)}, s32[64,2]{0,1:T(2,128)}, u32[]{:S(2)}) copy-start(s32[64,2]{0,1:T(2,128)} %param.39) | copy-start | bytes 1540
  27.8 103.8 %reduce-scatter.5.cloned.1.call-start = ((), (), s32[]{:S(2)}) async-start(), calls=%async_computation.5 | async-start | bytes 983040 | tf_op jit(solution)/shard_map/reduce_scatter | solution.py:118
  101.2 37.2 %copy-start.7 = (f32[64,2]{0,1:T(2,128)S(1)}, f32[64,2]{0,1:T(2,128)}, u32[]{:S(2)}) copy-start(f32[64,2]{0,1:T(2,128)} %param.40) | copy-start | bytes 1540
  131.6 12.9 %all-to-all-start.1 = ((bf16[512,8,24]{0,2,1:T(8,128)(2,1)}), bf16[512,8,24]{0,2,1:T(8,128)(2,1)S(1)}, u32[]{:S(2)}, u32[]{:S(2)}) async-start(bf16[512,8,24]{0,2,1:T(8,128)(2,1)} %bitcast.70), calls=%async_computation.3 | async-start | bytes 393216 | tf_op jit(solution)/shard_map/all_to_all | solution.py:127
Sparse Core Ops, SparseCore 0:
  27.9 24.6 reduce-scatter.2
  107.4 24.0 reduce-scatter.4
where the time goes:
time: 153 us; the launch traced here: 152 us
  blocking collectives  53.7 us (35%)
  waiting for transfers between devices  53 us (35%)
  matrix products  18.4 us (12%)
  between operations  14.3 us (9%)
  starting transfers between devices  4.69 us (3%)
  local copies, waits for them, and re-layouts  4.55 us (3%)
  other arithmetic  3.57 us (2%)
    all_to_all x1, blocking collectives, local(): lax.all_to_all(outbound.reshape(experts, slot_cap, model_width), 'ep', sp...  25.4 us
    reduce_scatter x1, waiting for transfers between devices, local(): lax.psum_scatter(lax.dot_general(down_local, hidden, (((0,), (1,)), ((),...  24.3 us
    reduce_scatter x1, waiting for transfers between devices, local(): lax.psum_scatter(partial_value.astype(jnp.bfloat16), 'tp', scatter_dimens...  22.9 us
    all_gather x1, blocking collectives, local(): lax.all_gather(mixed_in, 'tp', axis=1, tiled=True)  10.5 us
    all_gather x1, blocking collectives, local(): normed2 = lax.all_gather(own_cols, 'tp', axis=1, tiled=True)  8.93 us
    psum x1, blocking collectives, local(): squares = lax.psum(jnp.sum(part_values * part_values, axis=1), 'tp')  8.93 us
    dot_general x1, matrix products, local(): lax.dot_general(down_local, hidden, (((0,), (1,)), ((), ())), preferred_e...  6.1 us
    all_to_all x1, waiting for transfers between devices, local(): lax.all_to_all(back_rows, 'ep', split_axis=1, concat_axis=1, tiled=True)  5.74 us
  transfers between devices with their start and end apart: 3, of which 3 were waited for; matrix products, arithmetic and copies ran while one was open for 3% of the time, Pallas kernels for 0%

commit v1 on v0

v1 whole, which is shorter than its diff:
```python
import functools
import jax
import jax.numpy as jnp
from jax import lax
from jax.experimental import pallas as pl
from jax.experimental.pallas import tpu as pltpu
from jax.sharding import PartitionSpec as P

norm_eps = 1e-06
MESH = pl.DeviceIdType.MESH


def rms_scale(rows, gain):
    values = rows.astype(jnp.float32)
    scaled = values * lax.rsqrt(jnp.mean(values * values, axis=-1, keepdims=True) + norm_eps)
    return (scaled * gain).astype(jnp.bfloat16)


def state_step(
    inputs, state_re, state_im, decay_re, freq, log_step, in_re, in_im, out_re, out_im, skip
):
    highest = lax.Precision.HIGHEST
    step = jnp.exp(log_step)[:, None]
    magnitude = jnp.exp(decay_re * step)
    turn_re = magnitude * jnp.cos(freq * step)
    turn_im = magnitude * jnp.sin(freq * step)
    denom = decay_re * decay_re + freq * freq
    coef_re = ((turn_re - 1.0) * decay_re + turn_im * freq) / denom
    coef_im = (turn_im * decay_re - (turn_re - 1.0) * freq) / denom
    drive_re = jnp.einsum("sgh,ghp->sgp", inputs, in_re, preferred_element_type=jnp.float32)
    drive_im = jnp.einsum("sgh,ghp->sgp", inputs, in_im, preferred_element_type=jnp.float32)
    push_re = coef_re * drive_re - coef_im * drive_im
    push_im = coef_re * drive_im + coef_im * drive_re
    new_re = turn_re * state_re - turn_im * state_im + push_re
    new_im = turn_re * state_im + turn_im * state_re + push_im
    read = jnp.einsum("ghp,sgp->sgh", out_re.astype(jnp.float32), new_re, precision=highest)
    read = read - jnp.einsum("ghp,sgp->sgh", out_im.astype(jnp.float32), new_im, precision=highest)
    read = read + skip * inputs.astype(jnp.float32)
    return (read, new_re, new_im)


def remote(src, dst, send, recv, axis, peer):
    copy = pltpu.make_async_remote_copy(
        src_ref=src,
        dst_ref=dst,
        send_sem=send,
        recv_sem=recv,
        device_id={axis: peer},
        device_id_type=MESH,
    )
    copy.start()


def drain(ref, sem):
    pltpu.make_async_copy(ref, ref, sem).wait()


def near_first(index, count):
    half = (index + 1) // 2
    odd = index % 2
    return half * odd + (count - half) * (1 - odd)


def exchange(
    n_tp,
    n_ep,
    mixed_ref,
    tokens_ref,
    glu_ref,
    bias_ref,
    out_w_ref,
    gain_ref,
    select_ref,
    combine_ref,
    gate_hbm,
    up_hbm,
    down_hbm,
    out_ref,
    gate_w,
    up_w,
    down_w,
    ag_buf,
    rs_out,
    rs_in,
    disp,
    rows,
    xn,
    back_out,
    back_own,
    back_in,
    ret_out,
    ret_in,
    w_sem,
    ag_s,
    ag_r,
    rs_s,
    rs_r,
    disp_s,
    disp_r,
    fwd_s,
    fwd_r,
    back_s,
    back_r,
    ret_s,
    ret_r,
):
    tp = lax.axis_index("tp")
    ep = lax.axis_index("ep")
    seqs, chan = mixed_ref.shape
    width = out_ref.shape[1]
    groups = rows.shape[2]
    slots = n_ep * groups * 8
    hidden_n = gate_w.shape[1]
    f32 = jnp.float32
    bf16 = jnp.bfloat16

    loads = [
        pltpu.make_async_copy(src.at[0], dst, w_sem.at[i])
        for i, (src, dst) in enumerate(((gate_hbm, gate_w), (up_hbm, up_w), (down_hbm, down_w)))
    ]
    for load in loads:
        load.start()

    barrier = pltpu.get_barrier_semaphore()

    @pl.loop(1, n_tp)
    def _(k):
        pl.semaphore_signal(
            barrier, inc=1, device_id={"tp": lax.rem(tp + k, n_tp)}, device_id_type=MESH
        )

    @pl.loop(1, n_ep)
    def _(k):
        pl.semaphore_signal(
            barrier, inc=1, device_id={"ep": lax.rem(ep + k, n_ep)}, device_id_type=MESH
        )

    pl.semaphore_wait(barrier, n_tp + n_ep - 2)

    def peer_at(k):
        return lax.rem(tp + k, n_tp)

    def source_at(k):
        return lax.rem(tp + n_tp - k, n_tp)

    for k in range(1, n_tp):
        remote(mixed_ref, ag_buf.at[k - 1], ag_s.at[k - 1], ag_r.at[k - 1], "tp", peer_at(k))

    def glu_rows(owner):
        return glu_ref[pl.ds(pl.multiple_of(owner * chan, chan), chan), :]

    mixed = mixed_ref[...]
    gate = jnp.dot(mixed, glu_rows(tp), preferred_element_type=f32) + bias_ref[...]
    for k in range(1, n_tp):
        drain(ag_buf.at[k - 1], ag_r.at[k - 1])
        gate += jnp.dot(ag_buf[k - 1], glu_rows(source_at(k)), preferred_element_type=f32)
    gated = (mixed.astype(f32) * jax.nn.sigmoid(gate)).astype(bf16)

    def columns(owner):
        return pl.ds(pl.multiple_of(owner * width, width), width)

    for k in range(1, n_tp):
        part = jnp.dot(gated, out_w_ref[:, columns(peer_at(k))], preferred_element_type=f32)
        rs_out[k - 1] = part.astype(bf16)
        remote(
            rs_out.at[k - 1], rs_in.at[k - 1], rs_s.at[k - 1], rs_r.at[k - 1], "tp", peer_at(k)
        )
    total = jnp.dot(gated, out_w_ref[:, columns(tp)], preferred_element_type=f32)
    total = total.astype(bf16).astype(f32)
    for k in range(1, n_tp):
        drain(rs_in.at[k - 1], rs_r.at[k - 1])
        total += rs_in[k - 1].astype(f32)
    resid = (tokens_ref[:, columns(tp)].astype(f32) + total).astype(bf16)

    picked = jnp.dot(select_ref[...], resid, preferred_element_type=f32)
    disp[...] = picked.reshape(n_ep, groups, 8, width).astype(bf16)

    @pl.loop(1, n_ep)
    def _(i):
        to = lax.rem(ep + near_first(i, n_ep), n_ep)
        remote(disp.at[to], rows.at[tp, ep], disp_s, disp_r.at[i - 1], "ep", to)

    rows[tp, ep] = disp[ep]

    def forward(block):
        for k in range(1, n_tp):
            here = rows.at[tp, block]
            remote(here, here, fwd_s.at[k - 1], fwd_r.at[k - 1], "tp", peer_at(k))

    for k in range(1, n_tp):
        remote(
            disp.at[ep], rows.at[tp, ep], fwd_s.at[k - 1], fwd_r.at[k - 1], "tp", peer_at(k)
        )

    @pl.loop(1, n_ep)
    def _(i):
        block = lax.rem(ep + n_ep - near_first(i, n_ep), n_ep)
        drain(rows.at[tp, block], disp_r.at[i - 1])
        forward(block)

    def row_values(owner):
        return rows[owner].astype(f32).reshape(slots, width)

    values = row_values(tp)
    squares = jnp.sum(values * values, axis=1, keepdims=True)
    for k in range(1, n_tp):
        drain(rows.at[source_at(k)], fwd_r.at[k - 1])
        values = row_values(source_at(k))
        squares += jnp.sum(values * values, axis=1, keepdims=True)
    scale = lax.rsqrt(squares / (n_tp * width) + norm_eps)
    for owner in range(n_tp):
        cols = pl.ds(owner * width, width)
        xn[:, cols] = (row_values(owner) * scale * gain_ref[:, cols]).astype(bf16)

    loads[0].wait()
    loads[1].wait()
    pieces = []
    for start in range(0, hidden_n, 256):
        cols = pl.ds(start, min(256, hidden_n - start))
        gate_h = jnp.dot(xn[...], gate_w[:, cols], preferred_element_type=f32)
        up_h = jnp.dot(xn[...], up_w[:, cols], preferred_element_type=f32)
        pieces.append((jax.nn.silu(gate_h) * up_h).astype(bf16))
    hidden = jnp.concatenate(pieces, axis=1)
    loads[2].wait()

    def down(owner):
        part = jnp.dot(hidden, down_w[:, columns(owner)], preferred_element_type=f32)
        return part.reshape(n_ep, groups, 8, width).astype(bf16)

    for k in range(1, n_tp):
        back_out[k - 1] = down(peer_at(k))

        @pl.loop(1, n_ep + 1)
        def _(i):
            block = lax.rem(ep + near_first(i, n_ep) * (i // n_ep * -1 + 1), n_ep)
            remote(
                back_out.at[k - 1, block],
                back_in.at[block, k - 1],
                back_s.at[k - 1],
                back_r.at[block],
                "tp",
                peer_at(k),
            )

    back_own[...] = down(tp)

    def settled(block):
        drain(back_in.at[block], back_r.at[block])
        result = back_own[block].astype(f32)
        for k in range(1, n_tp):
            result += back_in[block, k - 1].astype(f32)
        return result.astype(bf16)

    @pl.loop(1, n_ep)
    def _(i):
        to = lax.rem(ep + near_first(i, n_ep), n_ep)
        ret_out[to] = settled(to)
        remote(ret_out.at[to], ret_in.at[ep], ret_s, ret_r.at[i - 1], "ep", to)

    ret_in[ep] = settled(ep)

    @pl.loop(1, n_ep)
    def _(i):
        block = lax.rem(ep + n_ep - near_first(i, n_ep), n_ep)
        drain(ret_in.at[block], ret_r.at[i - 1])

    returned = ret_in[...].astype(f32).reshape(slots, width)
    expert_total = jnp.dot(
        combine_ref[...], returned, precision=lax.Precision.HIGHEST, preferred_element_type=f32
    )
    out_ref[...] = (resid.astype(f32) + expert_total).astype(bf16)

    for k in range(1, n_tp):
        drain(mixed_ref, ag_s.at[k - 1])
        drain(rs_out.at[k - 1], rs_s.at[k - 1])
        drain(rows.at[0], fwd_s.at[k - 1])
        drain(back_out.at[k - 1], back_s.at[k - 1])
    drain(disp.at[pl.ds(0, n_ep - 1)], disp_s)
    drain(ret_out.at[pl.ds(0, n_ep - 1)], ret_s)


def local(
    tokens,
    mix_gain,
    w_in,
    decay_re,
    freq,
    log_step,
    in_re,
    in_im,
    out_re,
    out_im,
    skip,
    state_re,
    state_im,
    glu_weight,
    glu_bias,
    out_weight,
    ffn_gain,
    route,
    route_weight,
    expert_gate,
    expert_up,
    expert_down,
):
    seq_count, model_width = tokens.shape
    groups_local = decay_re.shape[0]
    n_tp = lax.axis_size("tp")
    experts = lax.axis_size("ep")
    local_width = model_width // n_tp
    top_count = route.shape[1]
    hidden_n = expert_gate.shape[2]
    slot_cap = (3 * seq_count * top_count + 2 * experts - 1) // (2 * experts)
    slot_rows = (slot_cap + 7) // 8 * 8
    slots = experts * slot_rows
    normed = rms_scale(tokens, mix_gain)
    drive = jnp.dot(normed, w_in, preferred_element_type=jnp.float32).astype(jnp.bfloat16)
    inputs = drive.reshape(seq_count, groups_local, -1)
    read, new_re, new_im = state_step(
        inputs, state_re, state_im, decay_re, freq, log_step, in_re, in_im, out_re, out_im, skip
    )
    mixed_in = jax.nn.gelu(read).reshape(seq_count, -1).astype(jnp.bfloat16)
    hits = (route[:, :, None] == jnp.arange(experts)[None, None, :]).astype(jnp.float32)
    earlier = jnp.tril(jnp.ones((seq_count, seq_count), jnp.float32), -1)
    before = jnp.dot(earlier, jnp.sum(hits, axis=1))
    rank = jnp.sum(before[:, None, :] * hits, axis=2).astype(jnp.int32)
    slot = route * slot_rows + rank
    picks = slot[:, :, None] == jnp.arange(slots)[None, None, :]
    combine = jnp.sum(jnp.where(picks, route_weight[:, :, None], 0.0), axis=1)
    select = jnp.any(slot.T[None, :, :] == jnp.arange(slots)[:, None, None], axis=1)
    chan = mixed_in.shape[1]
    block = (slot_rows // 8, 8, local_width)
    bf16 = jnp.bfloat16
    dma = pltpu.SemaphoreType.DMA
    vmem = pl.BlockSpec(memory_space=pltpu.VMEM)
    anyplace = pl.BlockSpec(memory_space=pl.ANY)
    mixed = pl.pallas_call(
        functools.partial(exchange, n_tp, experts),
        out_shape=jax.ShapeDtypeStruct((seq_count, local_width), bf16),
        in_specs=[vmem] * 8 + [anyplace] * 3,
        out_specs=vmem,
        scratch_shapes=[
            pltpu.VMEM((model_width, hidden_n), bf16),
            pltpu.VMEM((model_width, hidden_n), bf16),
            pltpu.VMEM((hidden_n, model_width), bf16),
            pltpu.VMEM((n_tp - 1, seq_count, chan), bf16),
            pltpu.VMEM((n_tp - 1, seq_count, local_width), bf16),
            pltpu.VMEM((n_tp - 1, seq_count, local_width), bf16),
            pltpu.VMEM((experts,) + block, bf16),
            pltpu.VMEM((n_tp, experts) + block, bf16),
            pltpu.VMEM((slots, model_width), bf16),
            pltpu.VMEM((n_tp - 1, experts) + block, bf16),
            pltpu.VMEM((experts,) + block, bf16),
            pltpu.VMEM((experts, n_tp - 1) + block, bf16),
            pltpu.VMEM((experts,) + block, bf16),
            pltpu.VMEM((experts,) + block, bf16),
            dma((3,)),
            dma((n_tp - 1,)),
            dma((n_tp - 1,)),
            dma((n_tp - 1,)),
            dma((n_tp - 1,)),
            dma,
            dma((experts - 1,)),
            dma((n_tp - 1,)),
            dma((n_tp - 1,)),
            dma((n_tp - 1,)),
            dma((experts,)),
            dma,
            dma((experts - 1,)),
        ],
        compiler_params=pltpu.CompilerParams(
            collective_id=0, has_side_effects=True, vmem_limit_bytes=40 * 1024 * 1024
        ),
    )(
        mixed_in,
        tokens,
        glu_weight,
        glu_bias[None, :],
        out_weight,
        ffn_gain[None, :],
        select.astype(bf16),
        combine,
        expert_gate,
        expert_up,
        expert_down,
    )
    return (mixed, new_re, new_im)


def solution(mesh):
    in_specs = (
        P("ep", None),
        P(),
        P(None, "tp"),
        P("tp", None),
        P("tp", None),
        P("tp"),
        P("tp", None, None),
        P("tp", None, None),
        P("tp", None, None),
        P("tp", None, None),
        P("tp", None),
        P("ep", "tp", None),
        P("ep", "tp", None),
        P(None, "tp"),
        P("tp"),
        P("tp", None),
        P(),
        P("ep", None),
        P("ep", None),
        P("ep", None, "tp"),
        P("ep", None, "tp"),
        P("ep", "tp", None),
    )
    out_specs = (P("ep", "tp"), P("ep", "tp", None), P("ep", "tp", None))
    return jax.shard_map(local, mesh=mesh, in_specs=in_specs, out_specs=out_specs, check_vma=False)
```

time: 153 us -> 63 us (0.41)
  blocking collectives: 53.7 us -> 0 us
  waiting for transfers between devices: 53 us -> 0 us
  Pallas kernels: 0 us -> 42.5 us
  between operations: 14.3 us -> 0.93 us
  matrix products: 18.4 us -> 5.5 us
  local copies, waits for them, and re-layouts: 4.55 us -> 10.1 us
  starting transfers between devices: 4.69 us -> 0 us
    reduce_scatter x2 -> x0, waiting for transfers between devices: 47.2 us -> none  [the longest x1 24.3 us: local(): lax.psum_scatter(lax.dot_general(down_local, hidden, (((0,), (1,)), ((),...]
    pallas_call x0 -> x1, Pallas kernels: none -> 42.5 us  [local(): pl.pallas_call(functools.partial(exchange, n_tp, experts), out_shape=jax....]
    all_to_all x1 -> x0, blocking collectives: 25.4 us -> none  [local(): lax.all_to_all(outbound.reshape(experts, slot_cap, model_width), 'ep', sp...]
    all_gather x2 -> x0, blocking collectives: 19.4 us -> none  [the longest x1 10.5 us: local(): lax.all_gather(mixed_in, 'tp', axis=1, tiled=True)]
    dot_general x6 -> x1, matrix products: 12.8 us -> 0.19 us  [local(): before = jnp.dot(earlier, jnp.sum(hits, axis=1))]
    psum x1 -> x0, blocking collectives: 8.93 us -> none  [local(): squares = lax.psum(jnp.sum(part_values * part_values, axis=1), 'tp')]
    unnamed x20 -> x33, local copies, waits for them, and re-layouts: 2.45 us -> 9 us
    all_to_all x1 -> x0, waiting for transfers between devices: 5.74 us -> none  [local(): lax.all_to_all(back_rows, 'ep', split_axis=1, concat_axis=1, tiled=True)]
  transfers between devices with their start and end apart: 3 -> 0, of which waited for: 3 -> 0; matrix products, arithmetic and copies ran while one was open for 3% -> 0% of each run, Pallas kernels for 0% -> 0%
where the time goes in v1:
time: 63 us; the launch traced here: 62.6 us
  Pallas kernels  42.5 us (67%)
  local copies, waits for them, and re-layouts  10.1 us (16%)
  matrix products  5.5 us (9%)
  other arithmetic  3.53 us (6%)
  between operations  0.93 us (1%)
    pallas_call x1, Pallas kernels, local(): pl.pallas_call(functools.partial(exchange, n_tp, experts), out_shape=jax....  42.5 us
    unnamed x33, local copies, waits for them, and re-layouts  9 us
    dot_general x1, matrix products, state_step(): jnp.einsum('sgh,ghp->sgp', inputs, in_re, preferred_element_type=jnp.floa...  1.81 us
    mul x1, other arithmetic, state_step(): turn_re = magnitude * jnp.cos(freq * step)  1.49 us
    dot_general x1, matrix products, local(): jnp.dot(normed, w_in, preferred_element_type=jnp.float32)  1.29 us

profile of v1, /device:TPU:0, one launch (start us, length us, event | category | flops | bytes accessed | tf_op | source)
XLA Modules:
  0.0 62.6 jit_solution(9045939558138406430)
XLA Ops:
  0.6 0.0 copy-start
  0.6 0.0 copy-start.4
  0.7 0.0 copy-start.11
  0.7 0.0 copy-start.13
  0.7 0.0 copy-start.8
  0.7 0.0 copy-start.7
  0.7 0.0 copy-start.6
  0.7 0.0 copy-start.5
  0.7 0.8 %exp.6 = f32[16]{0:T(128)S(1)} exponential(f32[16]{0:T(128)} %param.27) | non-fusion elementwise | bytes 128 | tf_op jit(solution)/shard_map/exp | solution.py:23
  1.5 1.5 %cosine_multiply_fusion = (f32[16,64]{1,0:T(8,128)}, f32[16,64]{1,0:T(8,128)}, f32[16,64]{1,0:T(8,128)}, f32[16,64]{1,0:T(8,128)}) fusion(f32[16,64]{1,0:T(8,128)} %param.26, f32[16,64]{1,0:T(8,128)} %param.25, f32[16]{0:T(128)S(1)} %exp.6), kind=kLoop, calls=%fused_computation.39 | loop fusion | flops 16384 | bytes 24640 | tf_op jit(solution)/shard_map/mul | solution.py:25
  3.0 1.1 %fusion.2 = f32[64]{0:T(128)S(1)} fusion(bf16[64,2048]{1,0:T(8,128)(2,1)} %tokens_ref.1), kind=kLoop, calls=%fused_computation.6 | loop fusion | flops 393152 | bytes 262400 | tf_op jit(solution)/shard_map/reduce_sum | solution.py:15
  4.1 0.0 copy-done
  4.2 1.3 %convolution_convert_fusion = bf16[64,256]{1,0:T(8,128)(2,1)S(1)} fusion(bf16[2048,256]{1,0:T(8,128)(2,1)S(1)} %copy-done, bf16[64,2048]{1,0:T(8,128)(2,1)} %tokens_ref.1, f32[2048]{0:T(1024)} %param.23, f32[64]{0:T(128)S(1)} %add_rsqrt_fusion), kind=kOutput, calls=%fused_computation.3 | convolution fusion | flops 67649536 | bytes 1351936 | tf_op jit(solution)/shard_map/dot_general | solution.py:317
  5.5 0.1 copy.62
  5.6 0.0 copy-start.12
  5.6 0.0 copy-start.14
  5.6 1.1 %fusion.25 = f32[16,64,64]{2,1,0:T(8,128)S(1)} fusion(bf16[64,16,16]{0,2,1:T(8,128)(2,1)S(1)} %bitcast.29, bf16[16,16,64]{2,1,0:T(8,128)(2,1)} %param.29), kind=kOutput, calls=%fused_computation.46 | convolution fusion | flops 2097152 | bytes 327680 | tf_op jit(solution)/shard_map/sgh,ghp->sgp/dot_general | solution.py:31
  6.7 1.8 %bitcast_add_fusion = (f32[64,16,64]{2,0,1:T(8,128)S(1)}, f32[64,16,64]{2,0,1:T(8,128)S(1)}) fusion(f32[16,64,64]{2,1,0:T(8,128)S(1)} %fusion.25, f32[64,16,64]{2,1,0:T(8,128)} %param.34, f32[64,16,64]{2,1,0:T(8,128)} %param.33, f32[16,64]{1,0:T(8,128)} %get-tuple-element.19, f32[16,64]{1,0:T(8,128)} %get-tuple-element.20, f32[16,64]{1,0:T(8,128)} %get-tuple-element.18, ...), kind=kOutput, calls=%fused_computation.9 | convolution fusion | flops 3014656 | bytes 1392640 | tf_op jit(solution)/shard_map/sgh,ghp->sgp/dot_general | solution.py:30
  8.6 0.0 copy-start.9
  8.6 0.0 copy-done.11
  8.6 0.5 fusion.26
  9.1 0.0 copy-done.12
  9.1 0.0 copy-done.14
  9.1 0.5 fusion.15
  9.7 0.0 copy-done.9
  9.7 0.1 copy.65.mixed_ref
  9.8 0.0 copy-done.13
  9.8 0.2 fusion.17
  10.0 0.1 fusion.16
  10.2 0.1 copy.66.select_ref
  10.3 0.8 %select_reduce_fusion.combine_ref = f32[64,192]{1,0:T(8,128)S(1)} fusion(f32[64,2]{0,1:T(2,128)} %param.40, s32[64,2]{0,1:T(2,128)S(1)} %convert_add_fusion), kind=kLoop, calls=%fused_computation.22 | loop fusion | flops 61440 | bytes 50176 | tf_op jit(solution)/shard_map/reduce_sum | solution.py:329
  11.1 0.0 copy-done.4
  11.1 0.0 copy-done.8
  11.1 0.0 copy-done.7
  11.1 0.0 copy-done.6
  11.1 0.0 copy-done.5
  11.1 0.0 copy-start.1
  11.1 2.0 %copy-done.1 = bf16[1,2048,896]{2,1,0:T(8,128)(2,1)S(1)} copy-done((bf16[1,2048,896]{2,1,0:T(8,128)(2,1)S(1)}, bf16[1,2048,896]{2,1,0:T(8,128)(2,1)}, u32[]{:S(2)}) %copy-start.1) | copy-done | bytes 3670040
  13.2 0.0 copy-start.2
  13.2 2.0 %copy-done.2 = bf16[1,2048,896]{2,1,0:T(8,128)(2,1)S(1)} copy-done((bf16[1,2048,896]{2,1,0:T(8,128)(2,1)S(1)}, bf16[1,2048,896]{2,1,0:T(8,128)(2,1)}, u32[]{:S(2)}) %copy-start.2) | copy-done | bytes 3670040
  15.2 0.0 copy-start.3
  15.2 2.0 %copy-done.3 = bf16[1,896,2048]{2,1,0:T(8,128)(2,1)S(1)} copy-done((bf16[1,896,2048]{2,1,0:T(8,128)(2,1)S(1)}, bf16[1,896,2048]{2,1,0:T(8,128)(2,1)}, u32[]{:S(2)}) %copy-start.3) | copy-done | bytes 3670040
  17.2 0.0 copy-start.10
  17.2 42.5 %shard_map.229 = bf16[64,512]{1,0:T(8,128)(2,1)S(1)} custom-call(bf16[64,256]{1,0:T(8,128)(2,1)S(1)} %copy.65.mixed_ref, bf16[64,2048]{1,0:T(8,128)(2,1)S(1)} %copy-done.4, bf16[1024,256]{1,0:T(8,128)(2,1)S(1)} %copy-done.6, f32[1,256]{1,0:T(1,128)S(1)} %bitcast.28, bf16[256,2048]{1,0:T(8,128)(2,1)S(1)} %copy-done.5, f32[1,2048]{1,0:T(1,128)S(1)} %bitcast.27, ...), custom_call_target="tpu_custom_call" | custom-call | tf_op jit(solution)/shard_map/pallas_call | solution.py:337
  59.7 0.0 copy-done.10
  59.7 1.1 %copy.67 = f32[64,16,64]{2,1,0:T(8,128)} copy(f32[64,16,64]{2,0,1:T(8,128)S(1)} %copy-done.10) | data formatting | bytes 524288
  60.8 1.1 %copy.68 = f32[64,16,64]{2,1,0:T(8,128)} copy(f32[64,16,64]{2,0,1:T(8,128)S(1)} %get-tuple-element.15) | data formatting | bytes 524288
  61.9 0.6 %copy.74 = bf16[64,512]{1,0:T(8,128)(2,1)} copy(bf16[64,512]{1,0:T(8,128)(2,1)S(1)} %shard_map.229) | data formatting | bytes 131072
  (6 shorter events, 0.0 us)
Async XLA Ops:
  0.6 3.5 %copy-start = (bf16[2048,256]{1,0:T(8,128)(2,1)S(1)}, bf16[2048,256]{1,0:T(8,128)(2,1)}, u32[]{:S(2)}) copy-start(bf16[2048,256]{1,0:T(8,128)(2,1)} %param.24) | copy-start | bytes 3145732
  0.6 10.4 %copy-start.4 = (bf16[64,2048]{1,0:T(8,128)(2,1)S(1)}, bf16[64,2048]{1,0:T(8,128)(2,1)}, u32[]{:S(2)}) copy-start(bf16[64,2048]{1,0:T(8,128)(2,1)} %tokens_ref.1) | copy-start | bytes 786436
  0.7 7.9 %copy-start.11 = (bf16[16,16,64]{2,1,0:T(8,128)(2,1)S(1)}, bf16[16,16,64]{2,1,0:T(8,128)(2,1)}, u32[]{:S(2)}) copy-start(bf16[16,16,64]{2,1,0:T(8,128)(2,1)} %param.30) | copy-start | bytes 98308
  0.7 9.1 %copy-start.13 = (s32[64,2]{0,1:T(2,128)S(1)}, s32[64,2]{0,1:T(2,128)}, u32[]{:S(2)}) copy-start(s32[64,2]{0,1:T(2,128)} %param.39) | copy-start | bytes 1540
  0.7 10.4 %copy-start.8 = (f32[256]{0:T(256)S(1)}, f32[256]{0:T(256)}, u32[]{:S(2)}) copy-start(f32[256]{0:T(256)} %param.36) | copy-start | bytes 3076
  0.7 10.4 %copy-start.7 = (f32[2048]{0:T(1024)S(1)}, f32[2048]{0:T(1024)}, u32[]{:S(2)}) copy-start(f32[2048]{0:T(1024)} %param.38) | copy-start | bytes 24580
  0.7 10.4 %copy-start.6 = (bf16[1024,256]{1,0:T(8,128)(2,1)S(1)}, bf16[1024,256]{1,0:T(8,128)(2,1)}, u32[]{:S(2)}) copy-start(bf16[1024,256]{1,0:T(8,128)(2,1)} %glu_ref.1) | copy-start | bytes 1572868
  0.7 10.4 %copy-start.5 = (bf16[256,2048]{1,0:T(8,128)(2,1)S(1)}, bf16[256,2048]{1,0:T(8,128)(2,1)}, u32[]{:S(2)}) copy-start(bf16[256,2048]{1,0:T(8,128)(2,1)} %out_w_ref.1) | copy-start | bytes 3145732
  5.6 3.5 %copy-start.12 = (bf16[16,16,64]{2,1,0:T(8,128)(2,1)S(1)}, bf16[16,16,64]{2,1,0:T(8,128)(2,1)}, u32[]{:S(2)}) copy-start(bf16[16,16,64]{2,1,0:T(8,128)(2,1)} %param.31) | copy-start | bytes 98308
  5.6 3.5 %copy-start.14 = (f32[16,16]{1,0:T(8,128)S(1)}, f32[16,16]{1,0:T(8,128)}, u32[]{:S(2)}) copy-start(f32[16,16]{1,0:T(8,128)} %param.32) | copy-start | bytes 3076
  8.6 1.1 %copy-start.9 = (f32[64,16,64]{2,0,1:T(8,128)}, f32[64,16,64]{2,0,1:T(8,128)S(1)}, u32[]{:S(2)}) copy-start(f32[64,16,64]{2,0,1:T(8,128)S(1)} %get-tuple-element.16) | copy-start | bytes 786436
  11.1 2.0 %copy-start.1 = (bf16[1,2048,896]{2,1,0:T(8,128)(2,1)S(1)}, bf16[1,2048,896]{2,1,0:T(8,128)(2,1)}, u32[]{:S(2)}) copy-start(bf16[1,2048,896]{2,1,0:T(8,128)(2,1)} %gate_hbm.1) | copy-start | bytes 11010052
  13.2 2.0 %copy-start.2 = (bf16[1,2048,896]{2,1,0:T(8,128)(2,1)S(1)}, bf16[1,2048,896]{2,1,0:T(8,128)(2,1)}, u32[]{:S(2)}) copy-start(bf16[1,2048,896]{2,1,0:T(8,128)(2,1)} %up_hbm.1) | copy-start | bytes 11010052
  15.2 2.0 %copy-start.3 = (bf16[1,896,2048]{2,1,0:T(8,128)(2,1)S(1)}, bf16[1,896,2048]{2,1,0:T(8,128)(2,1)}, u32[]{:S(2)}) copy-start(bf16[1,896,2048]{2,1,0:T(8,128)(2,1)} %down_hbm.1) | copy-start | bytes 11010052
  17.2 42.5 %copy-start.10 = (f32[64,16,64]{2,0,1:T(8,128)S(1)}, f32[64,16,64]{2,0,1:T(8,128)}, u32[]{:S(2)}) copy-start(f32[64,16,64]{2,0,1:T(8,128)} %copy-done.9) | copy-start | bytes 786436

commit v2 on v1

--- a/solution.py
+++ b/solution.py
@@ -14,29 +14,6 @@
     values = rows.astype(jnp.float32)
     scaled = values * lax.rsqrt(jnp.mean(values * values, axis=-1, keepdims=True) + norm_eps)
     return (scaled * gain).astype(jnp.bfloat16)
-
-
-def state_step(
-    inputs, state_re, state_im, decay_re, freq, log_step, in_re, in_im, out_re, out_im, skip
-):
-    highest = lax.Precision.HIGHEST
-    step = jnp.exp(log_step)[:, None]
-    magnitude = jnp.exp(decay_re * step)
-    turn_re = magnitude * jnp.cos(freq * step)
-    turn_im = magnitude * jnp.sin(freq * step)
-    denom = decay_re * decay_re + freq * freq
-    coef_re = ((turn_re - 1.0) * decay_re + turn_im * freq) / denom
-    coef_im = (turn_im * decay_re - (turn_re - 1.0) * freq) / denom
-    drive_re = jnp.einsum("sgh,ghp->sgp", inputs, in_re, preferred_element_type=jnp.float32)
-    drive_im = jnp.einsum("sgh,ghp->sgp", inputs, in_im, preferred_element_type=jnp.float32)
-    push_re = coef_re * drive_re - coef_im * drive_im
-    push_im = coef_re * drive_im + coef_im * drive_re
-    new_re = turn_re * state_re - turn_im * state_im + push_re
-    new_im = turn_re * state_im + turn_im * state_re + push_im
-    read = jnp.einsum("ghp,sgp->sgh", out_re.astype(jnp.float32), new_re, precision=highest)
-    read = read - jnp.einsum("ghp,sgp->sgh", out_im.astype(jnp.float32), new_im, precision=highest)
-    read = read + skip * inputs.astype(jnp.float32)
-    return (read, new_re, new_im)
 
 
 def remote(src, dst, send, recv, axis, peer):
@@ -64,18 +41,36 @@
 def exchange(
     n_tp,
     n_ep,
-    mixed_ref,
     tokens_ref,
-    glu_ref,
+    mix_gain_ref,
+    w_in_ref,
+    decay_ref,
+    freq_ref,
+    log_step_ref,
+    in_re_ref,
+    in_im_ref,
+    out_re_ref,
+    out_im_ref,
+    skip_ref,
     bias_ref,
-    out_w_ref,
     gain_ref,
-    select_ref,
-    combine_ref,
+    route_ref,
+    weight_ref,
+    state_re_hbm,
+    state_im_hbm,
+    glu_hbm,
+    out_w_hbm,
     gate_hbm,
     up_hbm,
     down_hbm,
     out_ref,
+    new_re_hbm,
+    new_im_hbm,
+    state_re,
+    state_im,
+    mixed_ref,
+    glu_ref,
+    out_w_ref,
     gate_w,
     up_w,
     down_w,
@@ -91,6 +86,8 @@
     ret_out,
     ret_in,
     w_sem,
+    state_sem,
+    new_sem,
     ag_s,
     ag_r,
     rs_s,
@@ -108,15 +105,30 @@
     ep = lax.axis_index("ep")
     seqs, chan = mixed_ref.shape
     width = out_ref.shape[1]
-    groups = rows.shape[2]
-    slots = n_ep * groups * 8
+    blocks = rows.shape[2]
+    slot_rows = blocks * 8
+    slots = n_ep * slot_rows
     hidden_n = gate_w.shape[1]
     f32 = jnp.float32
     bf16 = jnp.bfloat16
+    groups, places, entries = in_re_ref.shape
+
+    @pl.loop(0, groups)
+    def _(g):
+        for i, (far, near) in enumerate(((state_re_hbm, state_re), (state_im_hbm, state_im))):
+            pltpu.make_async_copy(far.at[:, g, :], near.at[g], state_sem.at[i]).start()
 
     loads = [
-        pltpu.make_async_copy(src.at[0], dst, w_sem.at[i])
-        for i, (src, dst) in enumerate(((gate_hbm, gate_w), (up_hbm, up_w), (down_hbm, down_w)))
+        pltpu.make_async_copy(src, dst, w_sem.at[i])
+        for i, (src, dst) in enumerate(
+            (
+                (glu_hbm, glu_ref),
+                (out_w_hbm, out_w_ref),
+                (gate_hbm.at[0], gate_w),
+                (up_hbm.at[0], up_w),
+                (down_hbm.at[0], down_w),
+            )
+        )
     ]
     for load in loads:
         load.start()
@@ -135,6 +147,71 @@
             barrier, inc=1, device_id={"ep": lax.rem(ep + k, n_ep)}, device_id_type=MESH
         )
 
+    diagonal = lax.broadcasted_iota(jnp.int32, (groups, groups), 0)
+    diagonal = diagonal == lax.broadcasted_iota(jnp.int32, (groups, groups), 1)
+    log_step = jnp.sum(jnp.where(diagonal, log_step_ref[...], 0.0), axis=1, keepdims=True)
+    step = jnp.exp(log_step)
+    decay = decay_ref[...]
+    freq = freq_ref[...]
+    magnitude = jnp.exp(decay * step)
+    turn_re = magnitude * jnp.cos(freq * step)
+    turn_im = magnitude * jnp.sin(freq * step)
+    denom = decay * decay + freq * freq
+    coef_re = ((turn_re - 1.0) * decay + turn_im * freq) / denom
+    coef_im = (turn_im * decay - (turn_re - 1.0) * freq) / denom
+
+    def lane_group(shape):
+        lane = lax.broadcasted_iota(jnp.int32, shape, len(shape) - 1)
+        first = lax.broadcasted_iota(jnp.int32, shape, 0) * places
+        return (lane >= first) & (lane < first + places)
+
+    spread = lax.broadcasted_iota(jnp.int32, (places, chan), 1) % places
+    spread = spread == lax.broadcasted_iota(jnp.int32, (places, chan), 0)
+    skip = jnp.dot(
+        skip_ref[...],
+        spread.astype(f32),
+        precision=lax.Precision.HIGHEST,
+        preferred_element_type=f32,
+    )
+    skip = jnp.sum(jnp.where(lane_group((groups, chan)), skip, 0.0), axis=0, keepdims=True)
+
+    normed = rms_scale(tokens_ref[...], mix_gain_ref[...])
+    drive = jnp.dot(normed, w_in_ref[...], preferred_element_type=f32).astype(bf16)
+    own_group = lane_group((groups, seqs, chan))
+    apart = jnp.where(own_group, drive.astype(f32)[None], 0.0).astype(bf16)
+    apart = apart.reshape(groups * seqs, chan)
+
+    def driven(ref):
+        weight = ref[...].astype(f32).reshape(chan, entries).astype(bf16)
+        value = jnp.dot(apart, weight, preferred_element_type=f32)
+        return value.reshape(groups, seqs, entries)
+
+    drive_re, drive_im = driven(in_re_ref), driven(in_im_ref)
+    turn_re, turn_im = turn_re[:, None, :], turn_im[:, None, :]
+    coef_re, coef_im = coef_re[:, None, :], coef_im[:, None, :]
+    drain(state_re, state_sem.at[0])
+    drain(state_im, state_sem.at[1])
+    old_re, old_im = state_re[...], state_im[...]
+    new_re = turn_re * old_re - turn_im * old_im + (coef_re * drive_re - coef_im * drive_im)
+    new_im = turn_re * old_im + turn_im * old_re + (coef_re * drive_im + coef_im * drive_re)
+    state_re[...] = new_re
+    state_im[...] = new_im
+
+    def read_out(value, ref):
+        weight = ref[...].astype(f32).reshape(chan, entries).astype(bf16)
+        value = value.reshape(groups * seqs, entries)
+        high = value.astype(bf16)
+        low = (value - high.astype(f32)).astype(bf16)
+        dims = (((1,), (1,)), ((), ()))
+        total = lax.dot_general(high, weight, dims, preferred_element_type=f32)
+        return total + lax.dot_general(low, weight, dims, preferred_element_type=f32)
+
+    read = read_out(new_re, out_re_ref) - read_out(new_im, out_im_ref)
+    read = jnp.where(own_group, read.reshape(groups, seqs, chan), 0.0)
+    read = jnp.sum(read, axis=0) + skip * drive.astype(f32)
+    mixed = jax.nn.gelu(read).astype(bf16)
+    mixed_ref[...] = mixed
+
     pl.semaphore_wait(barrier, n_tp + n_ep - 2)
 
     def peer_at(k):
@@ -146,15 +223,40 @@
     for k in range(1, n_tp):
         remote(mixed_ref, ag_buf.at[k - 1], ag_s.at[k - 1], ag_r.at[k - 1], "tp", peer_at(k))
 
+    @pl.loop(0, groups)
+    def _(g):
+        for i, (near, far) in enumerate(((state_re, new_re_hbm), (state_im, new_im_hbm))):
+            pltpu.make_async_copy(near.at[g], far.at[:, g, :], new_sem.at[i]).start()
+
+    def one_hot(index, size):
+        return lax.broadcasted_iota(jnp.int32, (seqs, size), 1).astype(f32) == index
+
+    choices = [route_ref[:, k : k + 1].astype(f32) for k in range(route_ref.shape[1])]
+    hits = [one_hot(choice, n_ep).astype(f32) for choice in choices]
+    earlier = lax.broadcasted_iota(jnp.int32, (seqs, seqs), 1)
+    earlier = earlier < lax.broadcasted_iota(jnp.int32, (seqs, seqs), 0)
+    before = jnp.dot(
+        earlier.astype(f32).astype(bf16), sum(hits).astype(bf16), preferred_element_type=f32
+    )
+    select = jnp.zeros((seqs, slots), f32)
+    combine = jnp.zeros((seqs, slots), f32)
+    for k, choice in enumerate(choices):
+        rank = jnp.sum(before * hits[k], axis=1, keepdims=True)
+        pick = one_hot(choice * slot_rows + rank, slots)
+        select = jnp.where(pick, 1.0, select)
+        combine = jnp.where(pick, weight_ref[:, k : k + 1], combine)
+
     def glu_rows(owner):
         return glu_ref[pl.ds(pl.multiple_of(owner * chan, chan), chan), :]
 
-    mixed = mixed_ref[...]
+    loads[0].wait()
     gate = jnp.dot(mixed, glu_rows(tp), preferred_element_type=f32) + bias_ref[...]
     for k in range(1, n_tp):
         drain(ag_buf.at[k - 1], ag_r.at[k - 1])
         gate += jnp.dot(ag_buf[k - 1], glu_rows(source_at(k)), preferred_element_type=f32)
     gated = (mixed.astype(f32) * jax.nn.sigmoid(gate)).astype(bf16)
+
+    loads[1].wait()
 
     def columns(owner):
         return pl.ds(pl.multiple_of(owner * width, width), width)
@@ -172,8 +274,10 @@
         total += rs_in[k - 1].astype(f32)
     resid = (tokens_ref[:, columns(tp)].astype(f32) + total).astype(bf16)
 
-    picked = jnp.dot(select_ref[...], resid, preferred_element_type=f32)
-    disp[...] = picked.reshape(n_ep, groups, 8, width).astype(bf16)
+    picked = lax.dot_general(
+        select.astype(bf16), resid, (((0,), (0,)), ((), ())), preferred_element_type=f32
+    )
+    disp[...] = picked.reshape(n_ep, blocks, 8, width).astype(bf16)
 
     @pl.loop(1, n_ep)
     def _(i):
@@ -212,8 +316,8 @@
         cols = pl.ds(owner * width, width)
         xn[:, cols] = (row_values(owner) * scale * gain_ref[:, cols]).astype(bf16)
 
-    loads[0].wait()
-    loads[1].wait()
+    loads[2].wait()
+    loads[3].wait()
     pieces = []
     for start in range(0, hidden_n, 256):
         cols = pl.ds(start, min(256, hidden_n - start))
@@ -221,11 +325,11 @@
         up_h = jnp.dot(xn[...], up_w[:, cols], preferred_element_type=f32)
         pieces.append((jax.nn.silu(gate_h) * up_h).astype(bf16))
     hidden = jnp.concatenate(pieces, axis=1)
-    loads[2].wait()
+    loads[4].wait()
 
     def down(owner):
         part = jnp.dot(hidden, down_w[:, columns(owner)], preferred_element_type=f32)
-        return part.reshape(n_ep, groups, 8, width).astype(bf16)
+        return part.reshape(n_ep, blocks, 8, width).astype(bf16)
 
     for k in range(1, n_tp):
         back_out[k - 1] = down(peer_at(k))
@@ -264,10 +368,11 @@
         block = lax.rem(ep + n_ep - near_first(i, n_ep), n_ep)
         drain(ret_in.at[block], ret_r.at[i - 1])
 
-    returned = ret_in[...].astype(f32).reshape(slots, width)
-    expert_total = jnp.dot(
-        combine_ref[...], returned, precision=lax.Precision.HIGHEST, preferred_element_type=f32
-    )
+    returned = ret_in[...].astype(f32).reshape(slots, width).astype(bf16)
+    high = combine.astype(bf16)
+    low = (combine - high.astype(f32)).astype(bf16)
+    expert_total = jnp.dot(high, returned, preferred_element_type=f32)
+    expert_total += jnp.dot(low, returned, preferred_element_type=f32)
     out_ref[...] = (resid.astype(f32) + expert_total).astype(bf16)
 
     for k in range(1, n_tp):
@@ -277,6 +382,8 @@
         drain(back_out.at[k - 1], back_s.at[k - 1])
     drain(disp.at[pl.ds(0, n_ep - 1)], disp_s)
     drain(ret_out.at[pl.ds(0, n_ep - 1)], ret_s)
+    drain(state_re, new_sem.at[0])
+    drain(state_im, new_sem.at[1])
 
 
 def local(
@@ -313,33 +420,28 @@
     slot_cap = (3 * seq_count * top_count + 2 * experts - 1) // (2 * experts)
     slot_rows = (slot_cap + 7) // 8 * 8
     slots = experts * slot_rows
-    normed = rms_scale(tokens, mix_gain)
-    drive = jnp.dot(normed, w_in, preferred_element_type=jnp.float32).astype(jnp.bfloat16)
-    inputs = drive.reshape(seq_count, groups_local, -1)
-    read, new_re, new_im = state_step(
-        inputs, state_re, state_im, decay_re, freq, log_step, in_re, in_im, out_re, out_im, skip
-    )
-    mixed_in = jax.nn.gelu(read).reshape(seq_count, -1).astype(jnp.bfloat16)
-    hits = (route[:, :, None] == jnp.arange(experts)[None, None, :]).astype(jnp.float32)
-    earlier = jnp.tril(jnp.ones((seq_count, seq_count), jnp.float32), -1)
-    before = jnp.dot(earlier, jnp.sum(hits, axis=1))
-    rank = jnp.sum(before[:, None, :] * hits, axis=2).astype(jnp.int32)
-    slot = route * slot_rows + rank
-    picks = slot[:, :, None] == jnp.arange(slots)[None, None, :]
-    combine = jnp.sum(jnp.where(picks, route_weight[:, :, None], 0.0), axis=1)
-    select = jnp.any(slot.T[None, :, :] == jnp.arange(slots)[:, None, None], axis=1)
-    chan = mixed_in.shape[1]
+    chan = w_in.shape[1]
+    state_block = (groups_local, seq_count, state_re.shape[2])
     block = (slot_rows // 8, 8, local_width)
     bf16 = jnp.bfloat16
     dma = pltpu.SemaphoreType.DMA
     vmem = pl.BlockSpec(memory_space=pltpu.VMEM)
     anyplace = pl.BlockSpec(memory_space=pl.ANY)
-    mixed = pl.pallas_call(
+    return pl.pallas_call(
         functools.partial(exchange, n_tp, experts),
-        out_shape=jax.ShapeDtypeStruct((seq_count, local_width), bf16),
-        in_specs=[vmem] * 8 + [anyplace] * 3,
-        out_specs=vmem,
+        out_shape=(
+            jax.ShapeDtypeStruct((seq_count, local_width), bf16),
+            jax.ShapeDtypeStruct(state_re.shape, jnp.float32),
+            jax.ShapeDtypeStruct(state_im.shape, jnp.float32),
+        ),
+        in_specs=[vmem] * 15 + [anyplace] * 7,
+        out_specs=(vmem, anyplace, anyplace),
         scratch_shapes=[
+            pltpu.VMEM(state_block, jnp.float32),
+            pltpu.VMEM(state_block, jnp.float32),
+            pltpu.VMEM((seq_count, chan), bf16),
+            pltpu.VMEM(glu_weight.shape, bf16),
+            pltpu.VMEM(out_weight.shape, bf16),
             pltpu.VMEM((model_width, hidden_n), bf16),
             pltpu.VMEM((model_width, hidden_n), bf16),
             pltpu.VMEM((hidden_n, model_width), bf16),
@@ -354,7 +456,9 @@
             pltpu.VMEM((experts, n_tp - 1) + block, bf16),
             pltpu.VMEM((experts,) + block, bf16),
             pltpu.VMEM((experts,) + block, bf16),
-            dma((3,)),
+            dma((5,)),
+            dma((2,)),
+            dma((2,)),
             dma((n_tp - 1,)),
             dma((n_tp - 1,)),
             dma((n_tp - 1,)),
@@ -369,22 +473,32 @@
             dma((experts - 1,)),
         ],
         compiler_params=pltpu.CompilerParams(
-            collective_id=0, has_side_effects=True, vmem_limit_bytes=40 * 1024 * 1024
+            collective_id=0, has_side_effects=True, vmem_limit_bytes=61 * 1024 * 1024
         ),
     )(
-        mixed_in,
         tokens,
+        mix_gain[None, :],
+        w_in,
+        decay_re,
+        freq,
+        log_step[None, :],
+        in_re,
+        in_im,
+        out_re,
+        out_im,
+        skip,
+        glu_bias[None, :],
+        ffn_gain[None, :],
+        route,
+        route_weight,
+        state_re,
+        state_im,
         glu_weight,
-        glu_bias[None, :],
         out_weight,
-        ffn_gain[None, :],
-        select.astype(bf16),
-        combine,
         expert_gate,
         expert_up,
         expert_down,
     )
-    return (mixed, new_re, new_im)
 
 
 def solution(mesh):

time: 63 us -> 54.3 us (0.86)
  matrix products: 5.5 us -> 0 us
  other arithmetic: 3.53 us -> 0 us
  Pallas kernels: 42.5 us -> 45.3 us
  local copies, waits for them, and re-layouts: 10.1 us -> 7.97 us
    dot_general x6 -> x0, matrix products: 5.5 us -> none  [the longest x1 1.81 us: state_step(): jnp.einsum('sgh,ghp->sgp', inputs, in_re, preferred_element_type=jnp.floa...]
    pallas_call x1, Pallas kernels: 42.5 us -> 45.3 us  [local(): pl.pallas_call(functools.partial(exchange, n_tp, experts), out_shape=(jax...]
    reduce_sum x4 -> x0, other arithmetic: 1.92 us -> none  [the longest x1 1.1 us: rms_scale(): jnp.mean(values * values, axis=-1, keepdims=True) + norm_eps]
    mul x1 -> x0, other arithmetic: 1.49 us -> none  [state_step(): turn_re = magnitude * jnp.cos(freq * step)]
    unnamed x33 -> x5, local copies, waits for them, and re-layouts: 9 us -> 7.97 us
    exp x1 -> x0, local copies, waits for them, and re-layouts: 0.81 us -> none  [state_step(): step = jnp.exp(log_step)[:, None]]
where the time goes in v2:
time: 54.3 us; the launch traced here: 54 us
  Pallas kernels  45.3 us (83%)
  local copies, waits for them, and re-layouts  7.97 us (15%)
  between operations  0.64 us (1%)
    pallas_call x1, Pallas kernels, local(): pl.pallas_call(functools.partial(exchange, n_tp, experts), out_shape=(jax...  45.3 us
    unnamed x5, local copies, waits for them, and re-layouts  7.97 us

profile of v2, /device:TPU:0, one launch (start us, length us, event | category | flops | bytes accessed | tf_op | source)
XLA Modules:
  0.0 54.0 jit_solution(7665777162253775024)
XLA Ops:
  0.6 1.4 %copy.25.route_ref = s32[64,2]{1,0:T(8,128)} copy(s32[64,2]{0,1:T(2,128)} %param.39) | data formatting | bytes 1024 | tf_op args[17]
  2.0 1.4 %copy.26.weight_ref = f32[64,2]{1,0:T(8,128)} copy(f32[64,2]{0,1:T(2,128)} %param.40) | data formatting | bytes 1024 | tf_op args[18]
  3.4 45.3 %shard_map.229 = (bf16[64,512]{1,0:T(8,128)(2,1)}, f32[64,16,64]{2,1,0:T(8,128)}, f32[64,16,64]{2,1,0:T(8,128)}) custom-call(bf16[64,2048]{1,0:T(8,128)(2,1)} %tokens_ref.1, f32[1,2048]{1,0:T(1,128)} %bitcast.4, bf16[2048,256]{1,0:T(8,128)(2,1)} %w_in_ref.1, f32[16,64]{1,0:T(8,128)} %decay_ref.1, f32[16,64]{1,0:T(8,128)} %freq_ref.1, f32[1,16]{1,0:T(1,128)} %bitcast.7, ...), custom_call_target="tpu_custom_call" | custom-call | tf_op jit(solution)/shard_map/pallas_call | solution.py:430
  48.7 1.5 %copy.30 = bf16[64,512]{1,0:T(8,128)(2,1)} copy(bf16[64,512]{1,0:T(8,128)(2,1)} %get-tuple-element.6) | data formatting | bytes 131072
  50.2 1.9 %copy.31 = f32[64,16,64]{2,1,0:T(8,128)} copy(f32[64,16,64]{2,1,0:T(8,128)} %get-tuple-element.7) | data formatting | bytes 524288
  52.1 1.9 %copy.32 = f32[64,16,64]{2,1,0:T(8,128)} copy(f32[64,16,64]{2,1,0:T(8,128)} %get-tuple-element.8) | data formatting | bytes 524288

commit v3 on v1

v3 whole, which is shorter than its diff:
```python
import functools
import jax
import jax.numpy as jnp
from jax import lax
from jax.experimental import pallas as pl
from jax.experimental.pallas import tpu as pltpu
from jax.sharding import PartitionSpec as P

norm_eps = 1e-06
MESH = pl.DeviceIdType.MESH


def rms_scale(rows, gain):
    values = rows.astype(jnp.float32)
    scaled = values * lax.rsqrt(jnp.mean(values * values, axis=-1, keepdims=True) + norm_eps)
    return (scaled * gain).astype(jnp.bfloat16)


def state_kernel(
    tokens_ref,
    mix_gain_ref,
    w_in_ref,
    decay_ref,
    freq_ref,
    log_step_ref,
    in_re_ref,
    in_im_ref,
    out_re_ref,
    out_im_ref,
    skip_ref,
    state_re_hbm,
    state_im_hbm,
    mixed_ref,
    new_re_hbm,
    new_im_hbm,
    state_re,
    state_im,
    state_sem,
    new_sem,
):
    f32 = jnp.float32
    bf16 = jnp.bfloat16
    groups, places, entries = in_re_ref.shape
    seqs, chan = mixed_ref.shape

    @pl.loop(0, groups)
    def _(g):
        for i, (far, near) in enumerate(((state_re_hbm, state_re), (state_im_hbm, state_im))):
            pltpu.make_async_copy(far.at[:, g, :], near.at[g], state_sem.at[i]).start()

    diagonal = lax.broadcasted_iota(jnp.int32, (groups, groups), 0)
    diagonal = diagonal == lax.broadcasted_iota(jnp.int32, (groups, groups), 1)
    log_step = jnp.sum(jnp.where(diagonal, log_step_ref[...], 0.0), axis=1, keepdims=True)
    step = jnp.exp(log_step)
    decay = decay_ref[...]
    freq = freq_ref[...]
    magnitude = jnp.exp(decay * step)
    turn_re = magnitude * jnp.cos(freq * step)
    turn_im = magnitude * jnp.sin(freq * step)
    denom = decay * decay + freq * freq
    coef_re = ((turn_re - 1.0) * decay + turn_im * freq) / denom
    coef_im = (turn_im * decay - (turn_re - 1.0) * freq) / denom

    def lane_group(shape):
        lane = lax.broadcasted_iota(jnp.int32, shape, len(shape) - 1)
        first = lax.broadcasted_iota(jnp.int32, shape, 0) * places
        return (lane >= first) & (lane < first + places)

    spread = lax.broadcasted_iota(jnp.int32, (places, chan), 1) % places
    spread = spread == lax.broadcasted_iota(jnp.int32, (places, chan), 0)
    skip = jnp.dot(
        skip_ref[...],
        spread.astype(f32),
        precision=lax.Precision.HIGHEST,
        preferred_element_type=f32,
    )
    skip = jnp.sum(jnp.where(lane_group((groups, chan)), skip, 0.0), axis=0, keepdims=True)

    normed = rms_scale(tokens_ref[...], mix_gain_ref[...])
    drive = jnp.dot(normed, w_in_ref[...], preferred_element_type=f32).astype(bf16)
    own_group = lane_group((groups, seqs, chan))
    apart = jnp.where(own_group, drive.astype(f32)[None], 0.0).astype(bf16)
    apart = apart.reshape(groups * seqs, chan)

    def driven(ref):
        weight = ref[...].astype(f32).reshape(chan, entries).astype(bf16)
        value = jnp.dot(apart, weight, preferred_element_type=f32)
        return value.reshape(groups, seqs, entries)

    drive_re, drive_im = driven(in_re_ref), driven(in_im_ref)
    turn_re, turn_im = turn_re[:, None, :], turn_im[:, None, :]
    coef_re, coef_im = coef_re[:, None, :], coef_im[:, None, :]
    drain(state_re, state_sem.at[0])
    drain(state_im, state_sem.at[1])
    old_re, old_im = state_re[...], state_im[...]
    new_re = turn_re * old_re - turn_im * old_im + (coef_re * drive_re - coef_im * drive_im)
    new_im = turn_re * old_im + turn_im * old_re + (coef_re * drive_im + coef_im * drive_re)
    state_re[...] = new_re
    state_im[...] = new_im

    @pl.loop(0, groups)
    def _(g):
        for i, (near, far) in enumerate(((state_re, new_re_hbm), (state_im, new_im_hbm))):
            pltpu.make_async_copy(near.at[g], far.at[:, g, :], new_sem.at[i]).start()

    def read_out(value, ref):
        weight = ref[...].astype(f32).reshape(chan, entries).astype(bf16)
        value = value.reshape(groups * seqs, entries)
        high = value.astype(bf16)
        low = (value - high.astype(f32)).astype(bf16)
        dims = (((1,), (1,)), ((), ()))
        total = lax.dot_general(high, weight, dims, preferred_element_type=f32)
        return total + lax.dot_general(low, weight, dims, preferred_element_type=f32)

    read = read_out(new_re, out_re_ref) - read_out(new_im, out_im_ref)
    read = jnp.where(own_group, read.reshape(groups, seqs, chan), 0.0)
    read = jnp.sum(read, axis=0) + skip * drive.astype(f32)
    mixed = jax.nn.gelu(read).astype(bf16)
    mixed_ref[...] = mixed
    drain(state_re, new_sem.at[0])
    drain(state_im, new_sem.at[1])


def remote(src, dst, send, recv, axis, peer):
    copy = pltpu.make_async_remote_copy(
        src_ref=src,
        dst_ref=dst,
        send_sem=send,
        recv_sem=recv,
        device_id={axis: peer},
        device_id_type=MESH,
    )
    copy.start()


def drain(ref, sem):
    pltpu.make_async_copy(ref, ref, sem).wait()


def near_first(index, count):
    half = (index + 1) // 2
    odd = index % 2
    return half * odd + (count - half) * (1 - odd)


def exchange(
    n_tp,
    n_ep,
    mixed_ref,
    tokens_ref,
    bias_ref,
    gain_ref,
    route_ref,
    weight_ref,
    glu_hbm,
    out_w_hbm,
    gate_hbm,
    up_hbm,
    down_hbm,
    out_ref,
    glu_ref,
    out_w_ref,
    gate_w,
    up_w,
    down_w,
    ag_buf,
    rs_out,
    rs_in,
    disp,
    rows,
    xn,
    back_out,
    back_own,
    back_in,
    ret_out,
    ret_in,
    w_sem,
    ag_s,
    ag_r,
    rs_s,
    rs_r,
    disp_s,
    disp_r,
    fwd_s,
    fwd_r,
    back_s,
    back_r,
    ret_s,
    ret_r,
):
    tp = lax.axis_index("tp")
    ep = lax.axis_index("ep")
    seqs, chan = mixed_ref.shape
    width = out_ref.shape[1]
    blocks = rows.shape[2]
    slot_rows = blocks * 8
    slots = n_ep * slot_rows
    hidden_n = gate_w.shape[1]
    f32 = jnp.float32
    bf16 = jnp.bfloat16

    loads = [
        pltpu.make_async_copy(src, dst, w_sem.at[i])
        for i, (src, dst) in enumerate(
            (
                (glu_hbm, glu_ref),
                (out_w_hbm, out_w_ref),
                (gate_hbm.at[0], gate_w),
                (up_hbm.at[0], up_w),
                (down_hbm.at[0], down_w),
            )
        )
    ]
    for load in loads:
        load.start()

    barrier = pltpu.get_barrier_semaphore()

    @pl.loop(1, n_tp)
    def _(k):
        pl.semaphore_signal(
            barrier, inc=1, device_id={"tp": lax.rem(tp + k, n_tp)}, device_id_type=MESH
        )

    @pl.loop(1, n_ep)
    def _(k):
        pl.semaphore_signal(
            barrier, inc=1, device_id={"ep": lax.rem(ep + k, n_ep)}, device_id_type=MESH
        )

    pl.semaphore_wait(barrier, n_tp + n_ep - 2)

    def peer_at(k):
        return lax.rem(tp + k, n_tp)

    def source_at(k):
        return lax.rem(tp + n_tp - k, n_tp)

    for k in range(1, n_tp):
        remote(mixed_ref, ag_buf.at[k - 1], ag_s.at[k - 1], ag_r.at[k - 1], "tp", peer_at(k))

    def one_hot(index, size):
        return lax.broadcasted_iota(jnp.int32, (seqs, size), 1).astype(f32) == index

    row = lax.broadcasted_iota(jnp.int32, (seqs, seqs), 0)
    lane = lax.broadcasted_iota(jnp.int32, (seqs, seqs), 1)

    def upright(ref, k):
        value = ref[k : k + 1, :].astype(f32)
        return jnp.sum(jnp.where(row == lane, value, 0.0), axis=1, keepdims=True)

    choices = [upright(route_ref, k) for k in range(route_ref.shape[0])]
    hits = [one_hot(choice, n_ep).astype(f32) for choice in choices]
    earlier = jnp.where(lane < row, 1.0, 0.0).astype(bf16)
    before = jnp.dot(earlier, sum(hits).astype(bf16), preferred_element_type=f32)
    select = jnp.zeros((seqs, slots), f32)
    combine = jnp.zeros((seqs, slots), f32)
    for k, choice in enumerate(choices):
        rank = jnp.sum(before * hits[k], axis=1, keepdims=True)
        pick = one_hot(choice * slot_rows + rank, slots)
        select = jnp.where(pick, 1.0, select)
        combine = jnp.where(pick, upright(weight_ref, k), combine)

    mixed = mixed_ref[...]

    def glu_rows(owner):
        return glu_ref[pl.ds(pl.multiple_of(owner * chan, chan), chan), :]

    loads[0].wait()
    gate = jnp.dot(mixed, glu_rows(tp), preferred_element_type=f32) + bias_ref[...]
    for k in range(1, n_tp):
        drain(ag_buf.at[k - 1], ag_r.at[k - 1])
        gate += jnp.dot(ag_buf[k - 1], glu_rows(source_at(k)), preferred_element_type=f32)
    gated = (mixed.astype(f32) * jax.nn.sigmoid(gate)).astype(bf16)

    loads[1].wait()

    def columns(owner):
        return pl.ds(pl.multiple_of(owner * width, width), width)

    for k in range(1, n_tp):
        part = jnp.dot(gated, out_w_ref[:, columns(peer_at(k))], preferred_element_type=f32)
        rs_out[k - 1] = part.astype(bf16)
        remote(
            rs_out.at[k - 1], rs_in.at[k - 1], rs_s.at[k - 1], rs_r.at[k - 1], "tp", peer_at(k)
        )
    total = jnp.dot(gated, out_w_ref[:, columns(tp)], preferred_element_type=f32)
    total = total.astype(bf16).astype(f32)
    for k in range(1, n_tp):
        drain(rs_in.at[k - 1], rs_r.at[k - 1])
        total += rs_in[k - 1].astype(f32)
    resid = (tokens_ref[:, columns(tp)].astype(f32) + total).astype(bf16)

    picked = lax.dot_general(
        select.astype(bf16), resid, (((0,), (0,)), ((), ())), preferred_element_type=f32
    )
    disp[...] = picked.reshape(n_ep, blocks, 8, width).astype(bf16)

    @pl.loop(1, n_ep)
    def _(i):
        to = lax.rem(ep + near_first(i, n_ep), n_ep)
        remote(disp.at[to], rows.at[tp, i], disp_s, disp_r.at[i - 1], "ep", to)

    half = n_ep // 2
    for k in range(1, n_tp):
        remote(disp.at[ep], rows.at[tp, 0], fwd_s.at[k - 1], fwd_r.at[0, k - 1], "tp", peer_at(k))
    rows[tp, 0] = disp[ep]

    @pl.loop(1, n_ep)
    def _(i):
        here = rows.at[tp, i]
        drain(here, disp_r.at[i - 1])
        for k in range(1, n_tp):
            remote(here, here, fwd_s.at[k - 1], fwd_r.at[i // half, k - 1], "tp", peer_at(k))

    for part in range(2):
        span = pl.ds(part * half, half)

        def row_values(owner):
            return rows[owner, span].astype(f32).reshape(slots // 2, width)

        values = row_values(tp)
        squares = jnp.sum(values * values, axis=1, keepdims=True)
        for k in range(1, n_tp):
            drain(rows.at[source_at(k), span], fwd_r.at[part, k - 1])
            values = row_values(source_at(k))
            squares += jnp.sum(values * values, axis=1, keepdims=True)
        scale = lax.rsqrt(squares / (n_tp * width) + norm_eps)
        for owner in range(n_tp):
            cols = pl.ds(owner * width, width)
            xn[:, cols] = (row_values(owner) * scale * gain_ref[:, cols]).astype(bf16)

        if part == 0:
            loads[2].wait()
            loads[3].wait()
        pieces = []
        for start in range(0, hidden_n, 256):
            cols = pl.ds(start, min(256, hidden_n - start))
            gate_h = jnp.dot(xn[...], gate_w[:, cols], preferred_element_type=f32)
            up_h = jnp.dot(xn[...], up_w[:, cols], preferred_element_type=f32)
            pieces.append((jax.nn.silu(gate_h) * up_h).astype(bf16))
        hidden = jnp.concatenate(pieces, axis=1)
        if part == 0:
            loads[4].wait()

        def down(owner):
            value = jnp.dot(hidden, down_w[:, columns(owner)], preferred_element_type=f32)
            return value.reshape(half, blocks, 8, width).astype(bf16)

        for k in range(1, n_tp):
            back_out[k - 1, span] = down(peer_at(k))

            @pl.loop(part * half, part * half + half)
            def _(i):
                remote(
                    back_out.at[k - 1, i],
                    back_in.at[i, k - 1],
                    back_s.at[k - 1],
                    back_r.at[i],
                    "tp",
                    peer_at(k),
                )

        back_own[span] = down(tp)

    def settled(i):
        drain(back_in.at[i], back_r.at[i])
        result = back_own[i].astype(f32)
        for k in range(1, n_tp):
            result += back_in[i, k - 1].astype(f32)
        return result.astype(bf16)

    @pl.loop(1, n_ep)
    def _(i):
        to = lax.rem(ep + n_ep - near_first(i, n_ep), n_ep)
        ret_out[to] = settled(i)
        remote(ret_out.at[to], ret_in.at[ep], ret_s, ret_r.at[i - 1], "ep", to)

    ret_in[ep] = settled(0)

    @pl.loop(1, n_ep)
    def _(i):
        block = lax.rem(ep + near_first(i, n_ep), n_ep)
        drain(ret_in.at[block], ret_r.at[i - 1])

    returned = ret_in[...].astype(f32).reshape(slots, width).astype(bf16)
    high = combine.astype(bf16)
    low = (combine - high.astype(f32)).astype(bf16)
    expert_total = jnp.dot(high, returned, preferred_element_type=f32)
    expert_total += jnp.dot(low, returned, preferred_element_type=f32)
    out_ref[...] = (resid.astype(f32) + expert_total).astype(bf16)

    for k in range(1, n_tp):
        drain(mixed_ref, ag_s.at[k - 1])
        drain(rs_out.at[k - 1], rs_s.at[k - 1])
        drain(rows.at[0], fwd_s.at[k - 1])
        drain(back_out.at[k - 1], back_s.at[k - 1])
    drain(disp.at[pl.ds(0, n_ep - 1)], disp_s)
    drain(ret_out.at[pl.ds(0, n_ep - 1)], ret_s)


def local(
    tokens,
    mix_gain,
    w_in,
    decay_re,
    freq,
    log_step,
    in_re,
    in_im,
    out_re,
    out_im,
    skip,
    state_re,
    state_im,
    glu_weight,
    glu_bias,
    out_weight,
    ffn_gain,
    route,
    route_weight,
    expert_gate,
    expert_up,
    expert_down,
):
    seq_count, model_width = tokens.shape
    groups_local = decay_re.shape[0]
    n_tp = lax.axis_size("tp")
    experts = lax.axis_size("ep")
    local_width = model_width // n_tp
    top_count = route.shape[1]
    hidden_n = expert_gate.shape[2]
    slot_cap = (3 * seq_count * top_count + 2 * experts - 1) // (2 * experts)
    slot_rows = (slot_cap + 7) // 8 * 8
    slots = experts * slot_rows
    chan = w_in.shape[1]
    state_block = (groups_local, seq_count, state_re.shape[2])
    block = (slot_rows // 8, 8, local_width)
    bf16 = jnp.bfloat16
    dma = pltpu.SemaphoreType.DMA
    vmem = pl.BlockSpec(memory_space=pltpu.VMEM)
    anyplace = pl.BlockSpec(memory_space=pl.ANY)
    mixed_in, new_re, new_im = pl.pallas_call(
        state_kernel,
        out_shape=(
            jax.ShapeDtypeStruct((seq_count, chan), bf16),
            jax.ShapeDtypeStruct(state_re.shape, jnp.float32),
            jax.ShapeDtypeStruct(state_im.shape, jnp.float32),
        ),
        in_specs=[vmem] * 11 + [anyplace] * 2,
        out_specs=(vmem, anyplace, anyplace),
        scratch_shapes=[
            pltpu.VMEM(state_block, jnp.float32),
            pltpu.VMEM(state_block, jnp.float32),
            dma((2,)),
            dma((2,)),
        ],
    )(
        tokens,
        mix_gain[None, :],
        w_in,
        decay_re,
        freq,
        log_step[None, :],
        in_re,
        in_im,
        out_re,
        out_im,
        skip,
        state_re,
        state_im,
    )
    mixed = pl.pallas_call(
        functools.partial(exchange, n_tp, experts),
        out_shape=jax.ShapeDtypeStruct((seq_count, local_width), bf16),
        in_specs=[vmem] * 6 + [anyplace] * 5,
        out_specs=vmem,
        scratch_shapes=[
            pltpu.VMEM(glu_weight.shape, bf16),
            pltpu.VMEM(out_weight.shape, bf16),
            pltpu.VMEM((model_width, hidden_n), bf16),
            pltpu.VMEM((model_width, hidden_n), bf16),
            pltpu.VMEM((hidden_n, model_width), bf16),
            pltpu.VMEM((n_tp - 1, seq_count, chan), bf16),
            pltpu.VMEM((n_tp - 1, seq_count, local_width), bf16),
            pltpu.VMEM((n_tp - 1, seq_count, local_width), bf16),
            pltpu.VMEM((experts,) + block, bf16),
            pltpu.VMEM((n_tp, experts) + block, bf16),
            pltpu.VMEM((slots // 2, model_width), bf16),
            pltpu.VMEM((n_tp - 1, experts) + block, bf16),
            pltpu.VMEM((experts,) + block, bf16),
            pltpu.VMEM((experts, n_tp - 1) + block, bf16),
            pltpu.VMEM((experts,) + block, bf16),
            pltpu.VMEM((experts,) + block, bf16),
            dma((5,)),
            dma((n_tp - 1,)),
            dma((n_tp - 1,)),
            dma((n_tp - 1,)),
            dma((n_tp - 1,)),
            dma,
            dma((experts - 1,)),
            dma((n_tp - 1,)),
            dma((2, n_tp - 1)),
            dma((n_tp - 1,)),
            dma((experts,)),
            dma,
            dma((experts - 1,)),
        ],
        compiler_params=pltpu.CompilerParams(
            collective_id=0, has_side_effects=True, vmem_limit_bytes=61 * 1024 * 1024
        ),
    )(
        mixed_in,
        tokens,
        glu_bias[None, :],
        ffn_gain[None, :],
        route.T,
        route_weight.T,
        glu_weight,
        out_weight,
        expert_gate,
        expert_up,
        expert_down,
    )
    return (mixed, new_re, new_im)


def solution(mesh):
    in_specs = (
        P("ep", None),
        P(),
        P(None, "tp"),
        P("tp", None),
        P("tp", None),
        P("tp"),
        P("tp", None, None),
        P("tp", None, None),
        P("tp", None, None),
        P("tp", None, None),
        P("tp", None),
        P("ep", "tp", None),
        P("ep", "tp", None),
        P(None, "tp"),
        P("tp"),
        P("tp", None),
        P(),
        P("ep", None),
        P("ep", None),
        P("ep", None, "tp"),
        P("ep", None, "tp"),
        P("ep", "tp", None),
    )
    out_specs = (P("ep", "tp"), P("ep", "tp", None), P("ep", "tp", None))
    return jax.shard_map(local, mesh=mesh, in_specs=in_specs, out_specs=out_specs, check_vma=False)
```

time: 63 us -> 47.1 us (0.75)
  local copies, waits for them, and re-layouts: 10.1 us -> 1.47 us
  matrix products: 5.5 us -> 0 us
  other arithmetic: 3.53 us -> 0 us
  Pallas kernels: 42.5 us -> 44.7 us
    unnamed x33 -> x1, local copies, waits for them, and re-layouts: 9 us -> 1.47 us
    dot_general x6 -> x0, matrix products: 5.5 us -> none  [the longest x1 1.81 us: state_step(): jnp.einsum('sgh,ghp->sgp', inputs, in_re, preferred_element_type=jnp.floa...]
    pallas_call x0 -> x1, Pallas kernels: none -> 4.61 us  [local(): pl.pallas_call(state_kernel, out_shape=(jax.ShapeDtypeStruct((seq_count,...]
    pallas_call x1, Pallas kernels: 42.5 us -> 40.1 us  [local(): pl.pallas_call(functools.partial(exchange, n_tp, experts), out_shape=jax....]
    reduce_sum x4 -> x0, other arithmetic: 1.92 us -> none  [the longest x1 1.1 us: rms_scale(): jnp.mean(values * values, axis=-1, keepdims=True) + norm_eps]
    mul x1 -> x0, other arithmetic: 1.49 us -> none  [state_step(): turn_re = magnitude * jnp.cos(freq * step)]
    exp x1 -> x0, local copies, waits for them, and re-layouts: 0.81 us -> none  [state_step(): step = jnp.exp(log_step)[:, None]]
where the time goes in v3:
time: 47.1 us; the launch traced here: 46.8 us
  Pallas kernels  44.7 us (95%)
  local copies, waits for them, and re-layouts  1.47 us (3%)
  between operations  0.65 us (1%)
    pallas_call x1, Pallas kernels, local(): pl.pallas_call(functools.partial(exchange, n_tp, experts), out_shape=jax....  40.1 us
    pallas_call x1, Pallas kernels, local(): pl.pallas_call(state_kernel, out_shape=(jax.ShapeDtypeStruct((seq_count,...  4.61 us
    unnamed x1, local copies, waits for them, and re-layouts  1.47 us

profile of v3, /device:TPU:0, one launch (start us, length us, event | category | flops | bytes accessed | tf_op | source)
XLA Modules:
  0.0 46.8 jit_solution(2826391118187089932)
XLA Ops:
  0.6 4.6 %shard_map.229 = (bf16[64,256]{1,0:T(8,128)(2,1)}, f32[64,16,64]{2,1,0:T(8,128)}, f32[64,16,64]{2,1,0:T(8,128)}) custom-call(bf16[64,2048]{1,0:T(8,128)(2,1)} %tokens_ref.3, f32[1,2048]{1,0:T(1,128)} %bitcast.6, bf16[2048,256]{1,0:T(8,128)(2,1)} %w_in_ref.1, f32[16,64]{1,0:T(8,128)} %decay_ref.1, f32[16,64]{1,0:T(8,128)} %freq_ref.1, f32[1,16]{1,0:T(1,128)} %bitcast.11, ...), custom_call_target="tpu_custom_call" | custom-call | tf_op jit(solution)/shard_map/pallas_call | solution.py:443
  5.3 40.1 %shard_map.230 = bf16[64,512]{1,0:T(8,128)(2,1)} custom-call(bf16[64,256]{1,0:T(8,128)(2,1)} %get-tuple-element.6.mixed_ref, bf16[64,2048]{1,0:T(8,128)(2,1)} %tokens_ref.3, f32[1,256]{1,0:T(1,128)} %bitcast.8, f32[1,2048]{1,0:T(1,128)} %bitcast.7, s32[2,64]{1,0:T(2,128)} %bitcast.9, f32[2,64]{1,0:T(2,128)} %bitcast.10, bf16[1024,256]{1,0:T(8,128)(2,1)} %glu_hbm.1, ...), custom_call_target="tpu_custom_call" | custom-call | tf_op jit(solution)/shard_map/pallas_call | solution.py:473
  45.3 1.5 %copy.26 = bf16[64,512]{1,0:T(8,128)(2,1)} copy(bf16[64,512]{1,0:T(8,128)(2,1)} %shard_map.230) | data formatting | bytes 131072
